TPU v7x, 32 devices: a whole 2x2x4 slice. The times are simulated.
32 devices in a mesh: ep: 16 (over z, y, x), tp: 2 (over core).
Axes of the slice: x: 2, y: 2, z: 4, core: 2. Of those that a mesh axis runs over, the one named last changes fastest.
Arguments:
- residual: bfloat16 [1024, 2048], P('ep', 'tp'), may hold values from -100 to 100
- route_ids: int32 [1024, 4], P('ep'), may hold values from 0 to 15, all different within a row; in each aligned block of 64 rows (0 to 63, 64 to 127, ...) at most 24 rows name the same one
- route_weights: float32 [1024, 4], P('ep'), may hold values from 0.1 to 1
- carried_state: float32 [2, 1024, 4096], P(None, 'ep', 'tp'), may hold values from -6 to 6
- mix_gain: float32 [2048], replicated, may hold values from 0.1 to 1.9
- in_proj: bfloat16 [2048, 1024], P(None, 'tp'), may hold values from -0.125 to 0.125
- decay_rate: float32 [64, 64], P('tp'), may hold values from 0.1 to 2
- frequency: float32 [64, 64], P('tp'), may hold values from -3 to 3
- step_size: float32 [64], P('tp'), may hold values from 0.05 to 1
- input_map: float32 [2, 64, 64, 16], P(None, 'tp'), may hold values from -1.5 to 1.5
- output_matrix: float32 [2, 64, 16, 64], P(None, 'tp'), may hold values from -0.5 to 0.5
- passthrough_scale: float32 [1024], P('tp'), may hold values from -4 to 4
- out_gain: float32 [1024], replicated, may hold values from 0.1 to 1.9
- out_proj: bfloat16 [1024, 2048], P(None, 'tp'), may hold values from -0.1875 to 0.1875
- ffn_gain: float32 [2048], replicated, may hold values from 0.1 to 1.9
- w_gate: bfloat16 [16, 2048, 2048], P('ep', None, 'tp'), may hold values from -5 to 5
- w_up: bfloat16 [16, 2048, 2048], P('ep', None, 'tp'), may hold values from -5 to 5
- w_down: bfloat16 [16, 2048, 2048], P('ep', 'tp'), may hold values from -0.125 to 0.125
Outputs:
- updated: bfloat16 [1024, 2048], P('ep', 'tp')
- new_state: float32 [2, 1024, 4096], P(None, 'ep', 'tp')
Inputs may be any that keep to these rules, and one draw needn't show every extreme that they name: `route_ids`: each row names 4 different experts. Among the 64 rows of one device (aligned blocks) no expert is named more than 24 times, and in every draw some block names some expert exactly 24 times.
All inputs are finite; a program needn't handle non-finite values.
Results may differ from a plain program's by a relative error of at most 0.018.
Values may be sent and summed in bfloat16 or wider, within the bound.
A program may use at most 128 MiB of HBM per device.

v0:
```python
import functools
import jax
import jax.numpy as jnp
from jax import lax
from jax.experimental import pallas as pl
from jax.experimental.pallas import tpu as pltpu
from jax.sharding import PartitionSpec as P

epsilon = 1e-06
clamp_limit = 7.0
swish_alpha = 1.702


def discretize(decay_rate, frequency, step_size):
    rate_real = -decay_rate
    time_step = step_size[:, None]
    magnitude = jnp.exp(rate_real * time_step)
    phase_angle = frequency * time_step
    bar_real = magnitude * jnp.cos(phase_angle)
    bar_imag = magnitude * jnp.sin(phase_angle)
    denominator = rate_real * rate_real + frequency * frequency
    shifted = bar_real - 1.0
    coef_real = (shifted * rate_real + bar_imag * frequency) / denominator
    coef_imag = (bar_imag * rate_real - shifted * frequency) / denominator
    return (bar_real, bar_imag, coef_real, coef_imag)


def peer_of(index, offset):
    out = index
    bit = 1
    while bit <= offset:
        if offset & bit:
            out = out + bit * (1 - 2 * ((index // bit) % 2))
        bit *= 2
    return out


def gelu_tanh(value):
    inner = 0.7978845608028654 * (value + 0.044715 * value * value * value)
    return 0.5 * value * (1.0 + jnp.tanh(inner))


def row_squares(value):
    return jnp.sum(value * value, axis=1, keepdims=True)


def layer_kernel(
    peers,
    capacity,
    group_channels,
    residual_ref,
    taken_ref,
    combine_ref,
    mix_gain_ref,
    transition_ref,
    passthrough_ref,
    out_gain_ref,
    ffn_gain_ref,
    state_hbm,
    in_hbm,
    push_hbm,
    read_hbm,
    out_hbm,
    gate_hbm,
    up_hbm,
    down_hbm,
    out_ref,
    new_state_hbm,
    state_v,
    in_v,
    push_v,
    read_v,
    out_v,
    residual_other,
    mixer_own,
    mixer_other,
    after_ref,
    buffer_ref,
    gate_w,
    up_w,
    down_w,
    rows_own,
    rows_other,
    flat_own,
    flat_other,
    activation,
    part_send,
    part_recv,
    part_own,
    back_send,
    back_recv,
    weight_sem,
    mixer_sem,
    swap_send_sem,
    swap_recv_sem,
    go_send_sem,
    go_recv_sem,
    pair_send_sem,
    pair_recv_sem,
    part_send_sem,
    part_recv_sem,
    back_send_sem,
    back_recv_sem,
):
    me = lax.axis_index("ep")
    core = lax.axis_index("tp")
    half_width = residual_ref.shape[1]
    hidden = gate_w.shape[1]
    tile = 256
    mixer_copies = [
        pltpu.make_async_copy(source, target, mixer_sem.at[place])
        for place, (source, target) in enumerate(
            (
                (in_hbm, in_v),
                (push_hbm, push_v),
                (state_hbm, state_v),
                (read_hbm, read_v),
                (out_hbm, out_v),
            )
        )
    ]
    weights = [
        pltpu.make_async_copy(gate_hbm, gate_w, weight_sem.at[0]),
        pltpu.make_async_copy(up_hbm, up_w, weight_sem.at[1]),
        pltpu.make_async_copy(down_hbm, down_w, weight_sem.at[2]),
    ]
    for copy in mixer_copies:
        copy.start()
    barrier = pltpu.get_barrier_semaphore()
    for offset in range(1, peers):
        pl.semaphore_signal(
            barrier,
            inc=1,
            device_id=(peer_of(me, offset), core),
            device_id_type=pl.DeviceIdType.MESH,
        )
    pl.semaphore_signal(
        barrier, inc=1, device_id=(me, 1 - core), device_id_type=pl.DeviceIdType.MESH
    )
    pl.semaphore_wait(barrier, peers)

    def remote(source, target, send_sem, recv_sem, ep_index, tp_index):
        return pltpu.make_async_remote_copy(
            src_ref=source,
            dst_ref=target,
            send_sem=send_sem,
            recv_sem=recv_sem,
            device_id=(ep_index, tp_index),
            device_id_type=pl.DeviceIdType.MESH,
        )

    own_start = pl.multiple_of(core * half_width, half_width)
    other_start = pl.multiple_of((1 - core) * half_width, half_width)
    own_columns = pl.ds(own_start, half_width)
    other_columns = pl.ds(other_start, half_width)
    narrow = jnp.bfloat16
    swap_rows = remote(
        residual_ref, residual_other, swap_send_sem.at[0], swap_recv_sem.at[0], me, 1 - core
    )
    swap_rows.start()
    start_rows = residual_ref[...].astype(jnp.float32)
    gained = (start_rows * mix_gain_ref[:, own_columns]).astype(narrow)
    squares = row_squares(start_rows)
    mixer_copies[0].wait()
    channels_sum = jnp.dot(gained, in_v[own_columns, :], preferred_element_type=jnp.float32)
    swap_rows.wait_recv()
    other_rows = residual_other[...].astype(jnp.float32)
    gained = (other_rows * mix_gain_ref[:, other_columns]).astype(narrow)
    squares = squares + row_squares(other_rows)
    channels_sum = channels_sum + jnp.dot(
        gained, in_v[other_columns, :], preferred_element_type=jnp.float32
    )
    channels = (channels_sum * lax.rsqrt(squares / (2 * half_width) + epsilon)).astype(narrow)
    for copy in weights:
        copy.start()

    mixer_width = channels.shape[1]
    entries = push_v.shape[2]
    wide = 128
    groups = wide // group_channels
    block = groups * entries
    shape = (wide, block)
    inside = (
        lax.broadcasted_iota(jnp.int32, shape, 0) // group_channels
        == lax.broadcasted_iota(jnp.int32, shape, 1) // entries
    )

    def block_diagonal(source, part, start):
        values = source[part, start : start + wide, :]
        return jnp.where(inside, jnp.concatenate([values] * groups, axis=1), 0.0).astype(narrow)

    for copy in mixer_copies[1:4]:
        copy.wait()
    for place in range(mixer_width // wide):
        start = place * wide
        states = slice(place * block, (place + 1) * block)
        inputs = channels[:, start : start + wide]
        raw_real = jnp.dot(
            inputs, block_diagonal(push_v, 0, start), preferred_element_type=jnp.float32
        )
        raw_imag = jnp.dot(
            inputs, block_diagonal(push_v, 1, start), preferred_element_type=jnp.float32
        )
        bar_real, bar_imag = transition_ref[0:1, states], transition_ref[1:2, states]
        coef_real, coef_imag = transition_ref[2:3, states], transition_ref[3:4, states]
        old_real, old_imag = state_v[0, :, states], state_v[1, :, states]
        new_real = (
            bar_real * old_real - bar_imag * old_imag + coef_real * raw_real - coef_imag * raw_imag
        )
        new_imag = (
            bar_real * old_imag + bar_imag * old_real + coef_real * raw_imag + coef_imag * raw_real
        )
        state_v[0, :, states] = new_real
        state_v[1, :, states] = new_imag
        transposed = (((1,), (1,)), ((), ()))
        mixed = (
            lax.dot_general(
                new_real.astype(narrow),
                block_diagonal(read_v, 0, start),
                transposed,
                preferred_element_type=jnp.float32,
            )
            - lax.dot_general(
                new_imag.astype(narrow),
                block_diagonal(read_v, 1, start),
                transposed,
                preferred_element_type=jnp.float32,
            )
            + passthrough_ref[:, start : start + wide] * inputs.astype(jnp.float32)
        )
        mixer_own[:, start : start + wide] = gelu_tanh(mixed).astype(narrow)
    swap_mixed = remote(
        mixer_own, mixer_other, swap_send_sem.at[1], swap_recv_sem.at[1], me, 1 - core
    )
    swap_mixed.start()
    own_channels = pl.ds(pl.multiple_of(core * mixer_width, mixer_width), mixer_width)
    other_channels = pl.ds(pl.multiple_of((1 - core) * mixer_width, mixer_width), mixer_width)
    mine = mixer_own[...].astype(jnp.float32)
    squares = row_squares(mine)
    mixer_copies[4].wait()
    projected = jnp.dot(
        (mine * out_gain_ref[:, own_channels]).astype(narrow),
        out_v[own_channels, :],
        preferred_element_type=jnp.float32,
    )
    swap_mixed.wait_recv()
    others = mixer_other[...].astype(jnp.float32)
    squares = squares + row_squares(others)
    projected = projected + jnp.dot(
        (others * out_gain_ref[:, other_channels]).astype(narrow),
        out_v[other_channels, :],
        preferred_element_type=jnp.float32,
    )
    after_rows = (
        start_rows + projected * lax.rsqrt(squares / (2 * mixer_width) + epsilon)
    ).astype(narrow)
    after_ref[...] = after_rows
    quarter = peers // 4
    for place in range(4):
        slots = slice(place * quarter * capacity, (place + 1) * quarter * capacity)
        buffer_ref[place * quarter : (place + 1) * quarter] = (
            jnp.dot(taken_ref[slots, :], after_rows, preferred_element_type=jnp.float32)
            .reshape(quarter, capacity, half_width)
            .astype(narrow)
        )

    half = peers // 2
    outward = {}
    middle = half + half // 2
    chunks = ((half, middle), (0, half), (middle, peers))
    for offset in [one for span in chunks for one in range(*span) if one]:
        peer = peer_of(me, offset)
        outward[offset] = remote(
            buffer_ref.at[peer],
            rows_own.at[offset],
            go_send_sem.at[offset],
            go_recv_sem.at[offset],
            peer,
            core,
        )
        outward[offset].start()
    rows_own[0] = buffer_ref[me]
    state_out = pltpu.make_async_copy(state_v, new_state_hbm, mixer_sem.at[5])
    state_out.start()
    back = {}
    parts = []
    pairs = {}
    for chunk, (first, last) in enumerate(chunks):
        count = (last - first) * capacity
        for offset in range(first, last):
            if offset:
                outward[offset].wait_recv()
            source = rows_own.at[offset] if offset else buffer_ref.at[me]
            pairs[offset] = remote(
                source,
                rows_other.at[offset],
                pair_send_sem.at[offset],
                pair_recv_sem.at[offset],
                me,
                1 - core,
            )
            pairs[offset].start()
        own_rows = (
            rows_own[first:last]
            .astype(jnp.float32)
            .reshape(count, half_width)
        )
        for offset in range(first, last):
            pairs[offset].wait_recv()
        other_half = (
            rows_other[first:last]
            .astype(jnp.float32)
            .reshape(count, half_width)
        )
        row_scale = lax.rsqrt(
            (row_squares(own_rows) + row_squares(other_half)) / (2 * half_width) + epsilon
        )
        flat_own[0:count] = (own_rows * row_scale * ffn_gain_ref[:, own_columns]).astype(narrow)
        flat_other[0:count] = (other_half * row_scale * ffn_gain_ref[:, other_columns]).astype(narrow)
        if chunk == 0:
            weights[0].wait()
            weights[1].wait()

        def hidden_tile(step, carry, count=count):
            columns = pl.ds(pl.multiple_of(step * tile, tile), tile)

            def both(weight):
                return jnp.dot(
                    flat_own[0:count],
                    weight[pl.ds(own_start, half_width), columns],
                    preferred_element_type=jnp.float32,
                ) + jnp.dot(
                    flat_other[0:count],
                    weight[pl.ds(other_start, half_width), columns],
                    preferred_element_type=jnp.float32,
                )

            gated = jnp.minimum(both(gate_w), clamp_limit)
            raised = jnp.clip(both(up_w), -clamp_limit, clamp_limit) + 1.0
            activation[0:count, columns] = (
                raised * gated * (1.0 / (1.0 + jnp.exp(-swish_alpha * gated)))
            ).astype(jnp.bfloat16)
            return carry

        lax.fori_loop(0, hidden // tile, hidden_tile, 0)
        if chunk == 0:
            weights[2].wait()

        def down_tiles(start, target):
            def down_tile(step, carry, count=count):
                columns = pl.ds(pl.multiple_of(step * tile, tile), tile)
                source = pl.ds(pl.multiple_of(start + step * tile, tile), tile)
                target[0:count, columns] = jnp.dot(
                    activation[0:count], down_w[:, source], preferred_element_type=jnp.float32
                ).astype(jnp.bfloat16)
                return carry

            lax.fori_loop(0, half_width // tile, down_tile, 0)

        down_tiles(other_start, part_send.at[chunk])
        parts.append(
            remote(
                part_send.at[chunk, pl.ds(0, count)],
                part_recv.at[chunk, pl.ds(0, count)],
                part_send_sem.at[chunk],
                part_recv_sem.at[chunk],
                me,
                1 - core,
            )
        )
        parts[chunk].start()
        down_tiles(own_start, part_own)
        parts[chunk].wait_recv()
        back_send[first:last] = (
            (part_own[0:count].astype(jnp.float32) + part_recv[chunk, 0:count].astype(jnp.float32))
            .reshape(last - first, capacity, half_width)
            .astype(jnp.bfloat16)
        )
        for offset in range(first, last):
            if offset == 0:
                back_recv[me] = back_send[0]
                continue
            peer = peer_of(me, offset)
            back[offset] = remote(
                back_send.at[offset],
                back_recv.at[me],
                back_send_sem.at[offset],
                back_recv_sem.at[offset],
                peer,
                core,
            )
            back[offset].start()
    for offset in range(1, peers):
        back[offset].wait_recv()
    returned = (
        back_recv[...]
        .astype(jnp.float32)
        .reshape(peers * capacity, half_width)
        .astype(jnp.bfloat16)
    )
    high = combine_ref[...].astype(jnp.bfloat16)
    low = (combine_ref[...] - high.astype(jnp.float32)).astype(jnp.bfloat16)
    expert_sum = jnp.dot(high, returned, preferred_element_type=jnp.float32) + jnp.dot(
        low, returned, preferred_element_type=jnp.float32
    )
    out_ref[...] = (after_ref[...].astype(jnp.float32) + expert_sum).astype(jnp.bfloat16)
    for offset in range(1, peers):
        outward[offset].wait_send()
        back[offset].wait_send()
    for offset in range(peers):
        pairs[offset].wait_send()
    for copy in parts:
        copy.wait_send()
    state_out.wait()
    swap_rows.wait_send()
    swap_mixed.wait_send()


def layer_call(group_channels, peers, capacity, residual, *operands):
    state, in_proj, push_map, read_map, out_proj, w_gate, w_up, w_down = operands[7:]
    half_width = residual.shape[1]
    rows = peers // 2 * capacity
    narrow = jnp.bfloat16
    blocks = pltpu.VMEM((peers, capacity, half_width), narrow)
    flat = pltpu.VMEM((rows, half_width), narrow)
    mixer = pltpu.VMEM((residual.shape[0], in_proj.shape[1]), narrow)
    dma = pltpu.SemaphoreType.DMA
    vmem = pl.BlockSpec(memory_space=pltpu.VMEM)
    anywhere = pl.BlockSpec(memory_space=pl.ANY)
    return pl.pallas_call(
        functools.partial(layer_kernel, peers, capacity, group_channels),
        out_shape=(
            jax.ShapeDtypeStruct(residual.shape, narrow),
            jax.ShapeDtypeStruct(state.shape, jnp.float32),
        ),
        in_specs=[vmem] * 8 + [anywhere] * 8,
        out_specs=(vmem, anywhere),
        scratch_shapes=[
            pltpu.VMEM(state.shape, jnp.float32),
            pltpu.VMEM(in_proj.shape, narrow),
            pltpu.VMEM(push_map.shape, jnp.float32),
            pltpu.VMEM(read_map.shape, jnp.float32),
            pltpu.VMEM(out_proj.shape, narrow),
            pltpu.VMEM(residual.shape, narrow),
            mixer,
            mixer,
            pltpu.VMEM(residual.shape, narrow),
            blocks,
            pltpu.VMEM(w_gate.shape, narrow),
            pltpu.VMEM(w_up.shape, narrow),
            pltpu.VMEM(w_down.shape, narrow),
            blocks,
            blocks,
            flat,
            flat,
            pltpu.VMEM((rows, w_gate.shape[1]), narrow),
            pltpu.VMEM((3, rows, half_width), narrow),
            pltpu.VMEM((3, rows, half_width), narrow),
            flat,
            blocks,
            blocks,
            dma((3,)),
            dma((6,)),
            dma((2,)),
            dma((2,)),
            dma((peers,)),
            dma((peers,)),
            dma((peers,)),
            dma((peers,)),
            dma((3,)),
            dma((3,)),
            dma((peers,)),
            dma((peers,)),
        ],
        compiler_params=pltpu.CompilerParams(
            collective_id=0, has_side_effects=True, vmem_limit_bytes=56 * 1024 * 1024
        ),
    )(residual, *operands)


def local(
    residual,
    route_ids,
    route_weights,
    carried_state,
    mix_gain,
    in_proj,
    decay_rate,
    frequency,
    step_size,
    input_map,
    output_matrix,
    passthrough_scale,
    out_gain,
    out_proj,
    ffn_gain,
    w_gate,
    w_up,
    w_down,
):
    row_count, half_width = residual.shape
    top_count = route_ids.shape[1]
    local_experts = w_gate.shape[0]
    peer_count = lax.axis_size("ep")
    expert_count = local_experts * peer_count
    capacity = max(2, 3 * row_count * top_count // (2 * expert_count))
    capacity = -(-capacity // 8) * 8
    slot_iota = jnp.arange(expert_count * capacity, dtype=jnp.int32)
    lane_expert = slot_iota // capacity
    named = route_ids[:, :, None] == lane_expert[None, None, :]
    chosen = jnp.any(named, axis=1)
    lane_weight = jnp.sum(jnp.where(named, route_weights[:, :, None], 0.0), axis=1)
    row_iota = jnp.arange(row_count, dtype=jnp.int32)
    earlier = (row_iota[:, None] > row_iota[None, :]).astype(jnp.bfloat16)
    before = jnp.dot(
        earlier, chosen.astype(jnp.bfloat16), preferred_element_type=jnp.float32
    )
    taken = chosen & (before == (slot_iota % capacity).astype(jnp.float32)[None, :])
    combine = jnp.where(taken, lane_weight, 0.0)
    width = decay_rate.size
    transition = jnp.stack(
        [term.reshape(width) for term in discretize(decay_rate, frequency, step_size)]
    )
    push_map = jnp.swapaxes(input_map, 2, 3).reshape(2, -1, input_map.shape[2])
    read_map = output_matrix.reshape(2, -1, output_matrix.shape[3])
    updated, new_state = layer_call(
        input_map.shape[3],
        peer_count,
        capacity,
        residual,
        taken.astype(jnp.bfloat16).T,
        combine,
        mix_gain[None, :],
        transition,
        passthrough_scale[None, :],
        out_gain[None, :],
        ffn_gain[None, :],
        carried_state,
        in_proj,
        push_map,
        read_map,
        out_proj,
        w_gate[0],
        w_up[0],
        w_down[0],
    )
    return (updated, new_state)


def solution(mesh):
    placed = (
        P("ep", "tp"),
        P("ep", None),
        P("ep", None),
        P(None, "ep", "tp"),
        P(),
        P(None, "tp"),
        P("tp", None),
        P("tp", None),
        P("tp"),
        P(None, "tp", None, None),
        P(None, "tp", None, None),
        P("tp"),
        P(),
        P(None, "tp"),
        P(),
        P("ep", None, "tp"),
        P("ep", None, "tp"),
        P("ep", "tp", None),
    )
    return jax.shard_map(
        local,
        mesh=mesh,
        in_specs=placed,
        out_specs=(P("ep", "tp"), P(None, "ep", "tp")),
        check_vma=False,
    )
```

profile of v0, /device:TPU:0, one launch (start us, length us, event | category | flops | bytes accessed | tf_op | source)
XLA Modules:
  0.0 63.4 jit_solution(8063410608085032341)
XLA Ops:
  0.7 0.8 %compare_reduce_fusion = pred[64,384]{1,0:T(8,128)(4,1)S(1)} fusion(s32[384]{0:T(512)S(1)} %add_select_fusion, s32[64,4]{0,1:T(4,128)} %param.19), kind=kLoop, calls=%fused_computation.3 | loop fusion | flops 172032 | bytes 27136 | tf_op jit(solution)/shard_map/reduce_or | solution.py:511
  1.5 0.9 %cosine_multiply_fusion = (f32[32,64]{1,0:T(8,128)S(1)}, f32[32,64]{1,0:T(8,128)S(1)}, f32[32,64]{1,0:T(8,128)S(1)}, f32[32,64]{1,0:T(8,128)S(1)}) fusion(f32[32,64]{1,0:T(8,128)} %param.25, f32[32,64]{1,0:T(8,128)} %param.24, f32[32]{0:T(128)} %param.26), kind=kLoop, calls=%fused_computation.13 | loop fusion | flops 34816 | bytes 49280 | tf_op jit(solution)/shard_map/mul | solution.py:19
  2.4 0.1 stack_reshape.12
  2.4 0.1 stack_reshape.14
  2.5 0.1 stack_reshape.15
  2.6 0.1 stack_reshape.13
  2.7 0.6 %pad_maximum_fusion.transition_ref = f32[4,2048]{1,0:T(4,128)} fusion(f32[1,2048]{1,0:T(1,128)S(1)} %stack_reshape.15, f32[1,2048]{1,0:T(1,128)S(1)} %stack_reshape.14, f32[1,2048]{1,0:T(1,128)S(1)} %stack_reshape.13, f32[1,2048]{1,0:T(1,128)S(1)} %stack_reshape.12), kind=kLoop, calls=%fused_computation.7 | loop fusion | flops 24576 | bytes 65536 | tf_op jit(solution)/shard_map/stack | solution.py:521
  3.3 0.8 %fusion.1 = f32[64,384]{1,0:T(8,128)S(1)} fusion(f32[64,4]{0,1:T(4,128)} %param.20, s32[384]{0:T(512)S(1)} %add_select_fusion, s32[64,4]{0,1:T(4,128)} %param.19), kind=kLoop, calls=%fused_computation.4 | loop fusion | flops 270336 | bytes 101888 | tf_op jit(solution)/shard_map/reduce_sum | solution.py:512
  4.2 0.8 %broadcast_select_fusion = (f32[64,384]{1,0:T(8,128)}, pred[64,384]{1,0:T(8,128)(4,1)S(1)}) fusion(f32[64,384]{1,0:T(8,128)S(1)} %fusion.1, pred[64,384]{1,0:T(8,128)(4,1)S(1)} %compare_reduce_fusion, f32[384]{0:T(512)S(1)} %fusion.6), kind=kOutput, calls=%fused_computation.6 | convolution fusion | flops 3223552 | bytes 247296 | tf_op jit(solution)/shard_map/dot_general | solution.py:515
  5.0 0.8 %copy.23.taken_ref = bf16[384,64]{1,0:T(8,128)(2,1)} copy(bf16[384,64]{0,1:T(8,128)(2,1)S(1)} %convert_bitcast_fusion) | data formatting | bytes 98304 | tf_op jit(solution)/shard_map/convert_element_type | solution.py:531
  5.7 53.8 %shard_map.185 = (bf16[64,1024]{1,0:T(8,128)(2,1)}, f32[2,64,2048]{2,1,0:T(8,128)}) custom-call(bf16[64,1024]{1,0:T(8,128)(2,1)} %residual_ref.1, bf16[384,64]{1,0:T(8,128)(2,1)} %copy.23.taken_ref, f32[64,384]{1,0:T(8,128)} %get-tuple-element.6.combine_ref, f32[1,2048]{1,0:T(1,128)} %bitcast.19, f32[4,2048]{1,0:T(4,128)} %pad_maximum_fusion.transition_ref, ...), custom_call_target="tpu_custom_call" | custom-call | tf_op jit(solution)/shard_map/pallas_call | solution.py:430
  59.6 1.6 %copy.26 = bf16[64,1024]{1,0:T(8,128)(2,1)} copy(bf16[64,1024]{1,0:T(8,128)(2,1)} %get-tuple-element.10) | data formatting | bytes 262144
  61.1 2.3 %copy.27 = f32[2,64,2048]{2,1,0:T(8,128)} copy(f32[2,64,2048]{2,1,0:T(8,128)} %get-tuple-element.11) | data formatting | bytes 2097152
  (3 shorter events, 0.0 us)
where the time goes:
time: 63.8 us; the launch traced here: 63.4 us
  Pallas kernels  53.8 us (84%)
  local copies, waits for them, and re-layouts  4.93 us (8%)
  other arithmetic  3.2 us (5%)
  matrix products  0.79 us (1%)
  between operations  0.67 us (1%)
    pallas_call x1, Pallas kernels, layer_call(): pl.pallas_call(functools.partial(layer_kernel, peers, capacity, group_cha...  53.8 us
    unnamed x2, local copies, waits for them, and re-layouts  3.86 us

commit v1 on v0

--- a/solution.py
+++ b/solution.py
@@ -13,7 +13,7 @@
 
 def discretize(decay_rate, frequency, step_size):
     rate_real = -decay_rate
-    time_step = step_size[:, None]
+    time_step = step_size
     magnitude = jnp.exp(rate_real * time_step)
     phase_angle = frequency * time_step
     bar_real = magnitude * jnp.cos(phase_angle)
@@ -44,15 +44,63 @@
     return jnp.sum(value * value, axis=1, keepdims=True)
 
 
+def fill_transition(decay_ref, frequency_ref, step_ref, transition_ref):
+    groups, entries = decay_ref.shape
+    diagonal = lax.broadcasted_iota(jnp.int32, (groups, groups), 0) == lax.broadcasted_iota(
+        jnp.int32, (groups, groups), 1
+    )
+    steps = jnp.sum(jnp.where(diagonal, step_ref[...], 0.0), axis=1, keepdims=True)
+    shape = (groups, groups * entries)
+    inside = (
+        lax.broadcasted_iota(jnp.int32, shape, 0)
+        == lax.broadcasted_iota(jnp.int32, shape, 1) // entries
+    )
+    for place, term in enumerate(discretize(decay_ref[...], frequency_ref[...], steps)):
+        spread = jnp.concatenate([term] * groups, axis=1)
+        transition_ref[place : place + 1, :] = jnp.sum(
+            jnp.where(inside, spread, 0.0), axis=0, keepdims=True
+        )
+
+
+def fill_routes(capacity, ids_ref, route_weight_ref, taken_ref, combine_ref):
+    top_count, rows = ids_ref.shape
+    experts = taken_ref.shape[0] // capacity
+    expert_iota = lax.broadcasted_iota(jnp.int32, (experts, rows), 0)
+    chosen = jnp.zeros((experts, rows), jnp.float32)
+    weight = jnp.zeros((experts, rows), jnp.float32)
+    for choice in range(top_count):
+        named = ids_ref[choice : choice + 1, :] == expert_iota
+        chosen = jnp.where(named, 1.0, chosen)
+        weight = jnp.where(named, route_weight_ref[choice : choice + 1, :], weight)
+    earlier = jnp.where(
+        lax.broadcasted_iota(jnp.int32, (rows, rows), 0)
+        < lax.broadcasted_iota(jnp.int32, (rows, rows), 1),
+        1.0,
+        0.0,
+    ).astype(jnp.bfloat16)
+    before = jnp.dot(
+        chosen.astype(jnp.bfloat16), earlier, preferred_element_type=jnp.float32
+    )
+    slot = jnp.where(chosen > 0.0, before, -1.0)
+    slot_iota = lax.broadcasted_iota(jnp.int32, (capacity, rows), 0).astype(jnp.float32)
+    for expert in range(experts):
+        lines = slice(expert * capacity, (expert + 1) * capacity)
+        taken = slot[expert : expert + 1, :] == slot_iota
+        taken_ref[lines, :] = jnp.where(taken, 1.0, 0.0).astype(jnp.bfloat16)
+        combine_ref[lines, :] = jnp.where(taken, weight[expert : expert + 1, :], 0.0)
+
+
 def layer_kernel(
     peers,
     capacity,
     group_channels,
     residual_ref,
-    taken_ref,
-    combine_ref,
+    ids_ref,
+    route_weight_ref,
     mix_gain_ref,
-    transition_ref,
+    decay_ref,
+    frequency_ref,
+    step_ref,
     passthrough_ref,
     out_gain_ref,
     ffn_gain_ref,
@@ -65,7 +113,6 @@
     up_hbm,
     down_hbm,
     out_ref,
-    new_state_hbm,
     state_v,
     in_v,
     push_v,
@@ -75,6 +122,9 @@
     mixer_own,
     mixer_other,
     after_ref,
+    transition_ref,
+    taken_ref,
+    combine_ref,
     buffer_ref,
     gate_w,
     up_w,
@@ -137,6 +187,8 @@
     pl.semaphore_signal(
         barrier, inc=1, device_id=(me, 1 - core), device_id_type=pl.DeviceIdType.MESH
     )
+    fill_transition(decay_ref, frequency_ref, step_ref, transition_ref)
+    fill_routes(capacity, ids_ref, route_weight_ref, taken_ref, combine_ref)
     pl.semaphore_wait(barrier, peers)
 
     def remote(source, target, send_sem, recv_sem, ep_index, tp_index):
@@ -280,8 +332,6 @@
         )
         outward[offset].start()
     rows_own[0] = buffer_ref[me]
-    state_out = pltpu.make_async_copy(state_v, new_state_hbm, mixer_sem.at[5])
-    state_out.start()
     back = {}
     parts = []
     pairs = {}
@@ -400,9 +450,10 @@
     )
     high = combine_ref[...].astype(jnp.bfloat16)
     low = (combine_ref[...] - high.astype(jnp.float32)).astype(jnp.bfloat16)
-    expert_sum = jnp.dot(high, returned, preferred_element_type=jnp.float32) + jnp.dot(
-        low, returned, preferred_element_type=jnp.float32
-    )
+    over_slots = (((0,), (0,)), ((), ()))
+    expert_sum = lax.dot_general(
+        high, returned, over_slots, preferred_element_type=jnp.float32
+    ) + lax.dot_general(low, returned, over_slots, preferred_element_type=jnp.float32)
     out_ref[...] = (after_ref[...].astype(jnp.float32) + expert_sum).astype(jnp.bfloat16)
     for offset in range(1, peers):
         outward[offset].wait_send()
@@ -411,13 +462,12 @@
         pairs[offset].wait_send()
     for copy in parts:
         copy.wait_send()
-    state_out.wait()
     swap_rows.wait_send()
     swap_mixed.wait_send()
 
 
 def layer_call(group_channels, peers, capacity, residual, *operands):
-    state, in_proj, push_map, read_map, out_proj, w_gate, w_up, w_down = operands[7:]
+    state, in_proj, push_map, read_map, out_proj, w_gate, w_up, w_down = operands[9:]
     half_width = residual.shape[1]
     rows = peers // 2 * capacity
     narrow = jnp.bfloat16
@@ -430,13 +480,12 @@
     return pl.pallas_call(
         functools.partial(layer_kernel, peers, capacity, group_channels),
         out_shape=(
-            jax.ShapeDtypeStruct(residual.shape, narrow),
-            jax.ShapeDtypeStruct(state.shape, jnp.float32),
+            pltpu.VMEM(residual.shape, narrow),
+            pltpu.VMEM(state.shape, jnp.float32),
         ),
-        in_specs=[vmem] * 8 + [anywhere] * 8,
-        out_specs=(vmem, anywhere),
+        in_specs=[vmem] * 10 + [anywhere] * 8,
+        out_specs=(vmem, vmem),
         scratch_shapes=[
-            pltpu.VMEM(state.shape, jnp.float32),
             pltpu.VMEM(in_proj.shape, narrow),
             pltpu.VMEM(push_map.shape, jnp.float32),
             pltpu.VMEM(read_map.shape, jnp.float32),
@@ -445,6 +494,9 @@
             mixer,
             mixer,
             pltpu.VMEM(residual.shape, narrow),
+            pltpu.VMEM((4, state.shape[2]), jnp.float32),
+            pltpu.VMEM((peers * capacity, residual.shape[0]), narrow),
+            pltpu.VMEM((peers * capacity, residual.shape[0]), jnp.float32),
             blocks,
             pltpu.VMEM(w_gate.shape, narrow),
             pltpu.VMEM(w_up.shape, narrow),
@@ -460,7 +512,7 @@
             blocks,
             blocks,
             dma((3,)),
-            dma((6,)),
+            dma((5,)),
             dma((2,)),
             dma((2,)),
             dma((peers,)),
@@ -505,22 +557,6 @@
     expert_count = local_experts * peer_count
     capacity = max(2, 3 * row_count * top_count // (2 * expert_count))
     capacity = -(-capacity // 8) * 8
-    slot_iota = jnp.arange(expert_count * capacity, dtype=jnp.int32)
-    lane_expert = slot_iota // capacity
-    named = route_ids[:, :, None] == lane_expert[None, None, :]
-    chosen = jnp.any(named, axis=1)
-    lane_weight = jnp.sum(jnp.where(named, route_weights[:, :, None], 0.0), axis=1)
-    row_iota = jnp.arange(row_count, dtype=jnp.int32)
-    earlier = (row_iota[:, None] > row_iota[None, :]).astype(jnp.bfloat16)
-    before = jnp.dot(
-        earlier, chosen.astype(jnp.bfloat16), preferred_element_type=jnp.float32
-    )
-    taken = chosen & (before == (slot_iota % capacity).astype(jnp.float32)[None, :])
-    combine = jnp.where(taken, lane_weight, 0.0)
-    width = decay_rate.size
-    transition = jnp.stack(
-        [term.reshape(width) for term in discretize(decay_rate, frequency, step_size)]
-    )
     push_map = jnp.swapaxes(input_map, 2, 3).reshape(2, -1, input_map.shape[2])
     read_map = output_matrix.reshape(2, -1, output_matrix.shape[3])
     updated, new_state = layer_call(
@@ -528,10 +564,12 @@
         peer_count,
         capacity,
         residual,
-        taken.astype(jnp.bfloat16).T,
-        combine,
+        route_ids.T,
+        route_weights.T,
         mix_gain[None, :],
-        transition,
+        decay_rate,
+        frequency,
+        step_size[None, :],
         passthrough_scale[None, :],
         out_gain[None, :],
         ffn_gain[None, :],

time: 63.8 us -> 55.6 us (0.87)
  local copies, waits for them, and re-layouts: 4.93 us -> 1.63 us
  other arithmetic: 3.2 us -> 0 us
  matrix products: 0.79 us -> 0 us
    unnamed x2, local copies, waits for them, and re-layouts: 3.86 us -> 1.63 us
    mul x1 -> x0, other arithmetic: 0.89 us -> none  [discretize(): bar_real = magnitude * jnp.cos(phase_angle)]
    reduce_sum x1 -> x0, other arithmetic: 0.84 us -> none  [local(): jnp.sum(jnp.where(named, route_weights[:, :, None], 0.0), axis=1)]
    reduce_or x1 -> x0, other arithmetic: 0.8 us -> none  [local(): chosen = jnp.any(named, axis=1)]
    dot_general x1 -> x0, matrix products: 0.79 us -> none  [local(): jnp.dot(earlier, chosen.astype(jnp.bfloat16), preferred_element_type=jnp....]
    convert_element_type x1 -> x0, local copies, waits for them, and re-layouts: 0.75 us -> none  [local(): taken.astype(jnp.bfloat16)]
    pallas_call x1, Pallas kernels: 53.8 us -> 53.2 us  [layer_call(): pl.pallas_call(functools.partial(layer_kernel, peers, capacity, group_cha...]
where the time goes in v1:
time: 55.6 us; the launch traced here: 55.5 us
  Pallas kernels  53.2 us (96%)
  local copies, waits for them, and re-layouts  1.63 us (3%)
  between operations  0.65 us (1%)
    pallas_call x1, Pallas kernels, layer_call(): pl.pallas_call(functools.partial(layer_kernel, peers, capacity, group_cha...  53.2 us
    unnamed x2, local copies, waits for them, and re-layouts  1.63 us

profile of v1, /device:TPU:0, one launch (start us, length us, event | category | flops | bytes accessed | tf_op | source)
XLA Modules:
  0.0 55.5 jit_solution(8751237581169608492)
XLA Ops:
  0.6 53.2 %shard_map.185 = (bf16[64,1024]{1,0:T(8,128)(2,1)S(1)}, f32[2,64,2048]{2,1,0:T(8,128)S(1)}) custom-call(bf16[64,1024]{1,0:T(8,128)(2,1)} %residual_ref.1, s32[4,64]{1,0:T(4,128)} %bitcast.22, f32[4,64]{1,0:T(4,128)} %bitcast.23, f32[1,2048]{1,0:T(1,128)} %bitcast.19, f32[32,64]{1,0:T(8,128)} %decay_ref.1, f32[32,64]{1,0:T(8,128)} %frequency_ref.1, ...), custom_call_target="tpu_custom_call" | custom-call | tf_op jit(solution)/shard_map/pallas_call | solution.py:480
  53.8 0.7 %copy.22 = bf16[64,1024]{1,0:T(8,128)(2,1)} copy(bf16[64,1024]{1,0:T(8,128)(2,1)S(1)} %get-tuple-element.2) | data formatting | bytes 262144
  54.5 1.0 %copy.23 = f32[2,64,2048]{2,1,0:T(8,128)} copy(f32[2,64,2048]{2,1,0:T(8,128)S(1)} %get-tuple-element.3) | data formatting | bytes 2097152

commit v2 on v1

v2 whole, which is shorter than its diff:
```python
import functools
import jax
import jax.numpy as jnp
from jax import lax
from jax.experimental import pallas as pl
from jax.experimental.pallas import tpu as pltpu
from jax.sharding import PartitionSpec as P

epsilon = 1e-06
clamp_limit = 7.0
swish_alpha = 1.702


def discretize(decay_rate, frequency, step_size):
    rate_real = -decay_rate
    time_step = step_size
    magnitude = jnp.exp(rate_real * time_step)
    phase_angle = frequency * time_step
    bar_real = magnitude * jnp.cos(phase_angle)
    bar_imag = magnitude * jnp.sin(phase_angle)
    denominator = rate_real * rate_real + frequency * frequency
    shifted = bar_real - 1.0
    coef_real = (shifted * rate_real + bar_imag * frequency) / denominator
    coef_imag = (bar_imag * rate_real - shifted * frequency) / denominator
    return (bar_real, bar_imag, coef_real, coef_imag)


def peer_of(index, offset):
    out = index
    bit = 1
    while bit <= offset:
        if offset & bit:
            out = out + bit * (1 - 2 * ((index // bit) % 2))
        bit *= 2
    return out


def gelu_tanh(value):
    inner = 0.7978845608028654 * (value + 0.044715 * value * value * value)
    return 0.5 * value * (1.0 + jnp.tanh(inner))


def row_squares(value):
    return jnp.sum(value * value, axis=1, keepdims=True)


def fill_transition(decay_ref, frequency_ref, step_ref, transition_ref):
    groups, entries = decay_ref.shape
    diagonal = lax.broadcasted_iota(jnp.int32, (groups, groups), 0) == lax.broadcasted_iota(
        jnp.int32, (groups, groups), 1
    )
    steps = jnp.sum(jnp.where(diagonal, step_ref[...], 0.0), axis=1, keepdims=True)
    shape = (groups, groups * entries)
    inside = (
        lax.broadcasted_iota(jnp.int32, shape, 0)
        == lax.broadcasted_iota(jnp.int32, shape, 1) // entries
    )
    for place, term in enumerate(discretize(decay_ref[...], frequency_ref[...], steps)):
        spread = jnp.concatenate([term] * groups, axis=1)
        transition_ref[place : place + 1, :] = jnp.sum(
            jnp.where(inside, spread, 0.0), axis=0, keepdims=True
        )


def fill_routes(capacity, route, experts, taken_ref, combine_ref):
    top_count = route.shape[0] // 2
    count, rows = experts.shape
    chosen = jnp.zeros((count, rows), jnp.float32)
    weight = jnp.zeros((count, rows), jnp.float32)
    for choice in range(top_count):
        named = route[choice : choice + 1, :] == experts
        chosen = jnp.where(named, 1.0, chosen)
        weight = jnp.where(named, route[top_count + choice : top_count + choice + 1, :], weight)
    earlier = jnp.where(
        lax.broadcasted_iota(jnp.int32, (rows, rows), 0)
        < lax.broadcasted_iota(jnp.int32, (rows, rows), 1),
        1.0,
        0.0,
    ).astype(jnp.bfloat16)
    before = jnp.dot(
        chosen.astype(jnp.bfloat16), earlier, preferred_element_type=jnp.float32
    )
    slot = jnp.where(chosen > 0.0, before, -1.0)
    slot_iota = lax.broadcasted_iota(jnp.int32, (capacity, rows), 0).astype(jnp.float32)
    for expert in range(count):
        lines = slice(expert * capacity, (expert + 1) * capacity)
        taken = slot[expert : expert + 1, :] == slot_iota
        taken_ref[lines, :] = jnp.where(taken, 1.0, 0.0).astype(jnp.bfloat16)
        combine_ref[lines, :] = jnp.where(taken, weight[expert : expert + 1, :], 0.0)


def layer_kernel(
    floors,
    peers,
    capacity,
    group_channels,
    residual_ref,
    ids_ref,
    route_weight_ref,
    mix_gain_ref,
    decay_ref,
    frequency_ref,
    step_ref,
    passthrough_ref,
    out_gain_ref,
    ffn_gain_ref,
    state_hbm,
    in_hbm,
    push_hbm,
    read_hbm,
    out_hbm,
    gate_hbm,
    up_hbm,
    down_hbm,
    out_ref,
    state_v,
    in_v,
    push_v,
    read_v,
    out_v,
    residual_other,
    mixer_other,
    after_ref,
    transition_ref,
    routes,
    taken_ref,
    combine_ref,
    line_rows,
    line_mixed,
    row_buffer,
    mixed_buffer,
    row_slots,
    mixed_slots,
    mixed_other,
    mixed_flat,
    after_own,
    after_other,
    gate_w,
    up_w,
    down_w,
    flat,
    activation,
    part_send,
    part_recv,
    part_own,
    back_send,
    back_recv,
    sum_send,
    sum_recv,
    weight_sem,
    mixer_sem,
    swap_send_sem,
    swap_recv_sem,
    line_send_sem,
    line_recv_sem,
    pair_send_sem,
    pair_recv_sem,
    plane_send_sem,
    plane_recv_sem,
):
    me = lax.axis_index("ep")
    core = lax.axis_index("tp")
    half_width = residual_ref.shape[1]
    hidden = gate_w.shape[1]
    tile = 1024
    mixer_copies = [
        pltpu.make_async_copy(source, target, mixer_sem.at[place])
        for place, (source, target) in enumerate(
            (
                (in_hbm, in_v),
                (push_hbm, push_v),
                (state_hbm, state_v),
                (read_hbm, read_v),
                (out_hbm, out_v),
            )
        )
    ]
    weights = [
        pltpu.make_async_copy(gate_hbm, gate_w, weight_sem.at[0]),
        pltpu.make_async_copy(up_hbm, up_w, weight_sem.at[1]),
        pltpu.make_async_copy(down_hbm, down_w, weight_sem.at[2]),
    ]
    for copy in mixer_copies:
        copy.start()
    plane = peers // floors
    barrier = pltpu.get_barrier_semaphore()
    greeted = [one for one in range(1, plane)] + [one * plane for one in range(1, floors)]
    for offset in greeted:
        pl.semaphore_signal(
            barrier,
            inc=1,
            device_id=(peer_of(me, offset), core),
            device_id_type=pl.DeviceIdType.MESH,
        )
    pl.semaphore_signal(
        barrier, inc=1, device_id=(me, 1 - core), device_id_type=pl.DeviceIdType.MESH
    )
    row_count = residual_ref.shape[0]
    shape = (plane, row_count)
    experts = (
        me // plane * plane
        + jnp.bitwise_xor(lax.broadcasted_iota(jnp.int32, shape, 0), me % plane)
    ).astype(jnp.float32)
    routes[0] = jnp.concatenate(
        [ids_ref[...].astype(jnp.float32), route_weight_ref[...]], axis=0
    )
    fill_transition(decay_ref, frequency_ref, step_ref, transition_ref)
    fill_routes(capacity, routes[0], experts, taken_ref.at[0], combine_ref.at[0])
    pl.semaphore_wait(barrier, len(greeted) + 1)

    def remote(source, target, send_sem, recv_sem, ep_index, tp_index):
        return pltpu.make_async_remote_copy(
            src_ref=source,
            dst_ref=target,
            send_sem=send_sem,
            recv_sem=recv_sem,
            device_id=(ep_index, tp_index),
            device_id_type=pl.DeviceIdType.MESH,
        )

    own_start = pl.multiple_of(core * half_width, half_width)
    other_start = pl.multiple_of((1 - core) * half_width, half_width)
    own_columns = pl.ds(own_start, half_width)
    other_columns = pl.ds(other_start, half_width)
    narrow = jnp.bfloat16
    swap_rows = remote(
        residual_ref, residual_other, swap_send_sem.at[0], swap_recv_sem.at[0], me, 1 - core
    )
    swap_rows.start()
    line_copies = {}
    kinds = {"route": 0, "rows": 1, "mixed": 2, "sum": 3}

    def to_line(kind, source, target, step, toward=None):
        line_copies[kind, step] = remote(
            source,
            target,
            line_send_sem.at[kinds[kind], step],
            line_recv_sem.at[kinds[kind], step],
            peer_of(me, (toward or step) * plane),
            core,
        )
        line_copies[kind, step].start()

    passed_on = {2: (3, 1)} if floors == 4 else {}
    outer = list(range(floors - 1, 0, -1))
    for step in outer:
        to_line("route", routes.at[0], routes.at[step], step)
    for step in outer:
        if step not in passed_on:
            to_line("rows", residual_ref, line_rows.at[step], step)
    plane_copies = {}
    plane_kinds = {"rows": 0, "mixed": 1, "back": 2}

    def to_plane(kind, step, source, target):
        for turn in range(1, plane):
            plane_copies[kind, step, turn] = remote(
                source.at[step, turn],
                target.at[step, turn],
                plane_send_sem.at[plane_kinds[kind], step, turn],
                plane_recv_sem.at[plane_kinds[kind], step, turn],
                peer_of(me, turn),
                core,
            )
            plane_copies[kind, step, turn].start()
        target[step, 0] = source[step, 0]

    def from_plane(kind, step):
        for turn in range(1, plane):
            plane_copies[kind, step, turn].wait_recv()

    def hand_out(kind, step, values, buffer, target):
        buffer[step] = (
            jnp.dot(taken_ref[step], values, preferred_element_type=jnp.float32)
            .reshape(plane, capacity, values.shape[1])
            .astype(jnp.bfloat16)
        )
        to_plane(kind, step, buffer, target)

    start_rows = residual_ref[...].astype(jnp.float32)
    gained = (start_rows * mix_gain_ref[:, own_columns]).astype(narrow)
    squares = row_squares(start_rows)
    mixer_copies[0].wait()
    channels_sum = jnp.dot(gained, in_v[own_columns, :], preferred_element_type=jnp.float32)
    hand_out("rows", 0, residual_ref[...], row_buffer, row_slots)
    swap_rows.wait_recv()
    other_rows = residual_other[...].astype(jnp.float32)
    gained = (other_rows * mix_gain_ref[:, other_columns]).astype(narrow)
    squares = squares + row_squares(other_rows)
    channels_sum = channels_sum + jnp.dot(
        gained, in_v[other_columns, :], preferred_element_type=jnp.float32
    )
    channels = (channels_sum * lax.rsqrt(squares / (2 * half_width) + epsilon)).astype(narrow)
    for copy in weights:
        copy.start()

    mixer_width = channels.shape[1]
    entries = push_v.shape[2]
    wide = 128
    groups = wide // group_channels
    block = groups * entries
    shape = (wide, block)
    inside = (
        lax.broadcasted_iota(jnp.int32, shape, 0) // group_channels
        == lax.broadcasted_iota(jnp.int32, shape, 1) // entries
    )

    def block_diagonal(source, part, start):
        values = source[part, start : start + wide, :]
        return jnp.where(inside, jnp.concatenate([values] * groups, axis=1), 0.0).astype(narrow)

    for copy in mixer_copies[1:4]:
        copy.wait()
    for place in range(mixer_width // wide):
        start = place * wide
        states = slice(place * block, (place + 1) * block)
        inputs = channels[:, start : start + wide]
        raw_real = jnp.dot(
            inputs, block_diagonal(push_v, 0, start), preferred_element_type=jnp.float32
        )
        raw_imag = jnp.dot(
            inputs, block_diagonal(push_v, 1, start), preferred_element_type=jnp.float32
        )
        bar_real, bar_imag = transition_ref[0:1, states], transition_ref[1:2, states]
        coef_real, coef_imag = transition_ref[2:3, states], transition_ref[3:4, states]
        old_real, old_imag = state_v[0, :, states], state_v[1, :, states]
        new_real = (
            bar_real * old_real - bar_imag * old_imag + coef_real * raw_real - coef_imag * raw_imag
        )
        new_imag = (
            bar_real * old_imag + bar_imag * old_real + coef_real * raw_imag + coef_imag * raw_real
        )
        state_v[0, :, states] = new_real
        state_v[1, :, states] = new_imag
        transposed = (((1,), (1,)), ((), ()))
        mixed = (
            lax.dot_general(
                new_real.astype(narrow),
                block_diagonal(read_v, 0, start),
                transposed,
                preferred_element_type=jnp.float32,
            )
            - lax.dot_general(
                new_imag.astype(narrow),
                block_diagonal(read_v, 1, start),
                transposed,
                preferred_element_type=jnp.float32,
            )
            + passthrough_ref[:, start : start + wide] * inputs.astype(jnp.float32)
        )
        line_mixed[0, :, start : start + wide] = gelu_tanh(mixed).astype(narrow)
    for step in outer:
        to_line("mixed", line_mixed.at[0], line_mixed.at[step], step)
    swap_mixed = remote(
        line_mixed.at[0], mixer_other, swap_send_sem.at[1], swap_recv_sem.at[1], me, 1 - core
    )
    swap_mixed.start()
    hand_out("mixed", 0, line_mixed[0], mixed_buffer, mixed_slots)
    own_channels = pl.ds(pl.multiple_of(core * mixer_width, mixer_width), mixer_width)
    other_channels = pl.ds(pl.multiple_of((1 - core) * mixer_width, mixer_width), mixer_width)

    def after_mixer(rows, mine, others):
        count = rows.shape[0]
        squares = row_squares(mine) + row_squares(others)
        mixed_flat[0:count, own_channels] = (mine * out_gain_ref[:, own_channels]).astype(narrow)
        mixed_flat[0:count, other_channels] = (
            others * out_gain_ref[:, other_channels]
        ).astype(narrow)
        projected = jnp.dot(
            mixed_flat[0:count], out_v[...], preferred_element_type=jnp.float32
        )
        return (rows + projected * lax.rsqrt(squares / (2 * mixer_width) + epsilon)).astype(
            narrow
        )

    def relay_rows(step):
        line_copies["route", step].wait_recv()
        fill_routes(capacity, routes[step], experts, taken_ref.at[step], combine_ref.at[step])
        line_copies["rows", step].wait_recv()
        for late, (source, toward) in passed_on.items():
            if source == step:
                to_line("rows", line_rows.at[source], line_rows.at[late], late, toward)
        hand_out("rows", step, line_rows[step], row_buffer, row_slots)

    def relay_mixed(step):
        line_copies["mixed", step].wait_recv()
        hand_out("mixed", step, line_mixed[step], mixed_buffer, mixed_slots)

    prompt = [step for step in range(1, floors) if step not in passed_on]
    for step in prompt:
        relay_rows(step)
    mixer_copies[4].wait()
    swap_mixed.wait_recv()
    after_ref[...] = after_mixer(
        start_rows, line_mixed[0].astype(jnp.float32), mixer_other[...].astype(jnp.float32)
    )
    for step in prompt:
        relay_mixed(step)
    for step in passed_on:
        relay_rows(step)
        relay_mixed(step)

    pairs = {}
    slots = plane * capacity

    def to_pair(kind, place, source, target):
        pairs[kind, place] = remote(
            source,
            target,
            pair_send_sem.at[kind, place],
            pair_recv_sem.at[kind, place],
            me,
            1 - core,
        )
        pairs[kind, place].start()

    def share_mixed(step):
        from_plane("mixed", step)
        to_pair(0, step, mixed_slots.at[step], mixed_other.at[step])

    def project(step):
        pairs[0, step].wait_recv()
        from_plane("rows", step)
        after_own[step] = after_mixer(
            row_slots[step].astype(jnp.float32).reshape(slots, half_width),
            mixed_slots[step].astype(jnp.float32).reshape(slots, mixer_width),
            mixed_other[step].astype(jnp.float32).reshape(slots, mixer_width),
        )
        to_pair(1, step, after_own.at[step], after_other.at[step])

    def apply_expert(chunk, first, last):
        count = (last - first) * slots
        for step in range(first, last):
            pairs[1, step].wait_recv()
        own_rows = after_own[first:last].astype(jnp.float32).reshape(count, half_width)
        other_half = after_other[first:last].astype(jnp.float32).reshape(count, half_width)
        row_scale = lax.rsqrt(
            (row_squares(own_rows) + row_squares(other_half)) / (2 * half_width) + epsilon
        )
        flat[0:count, own_columns] = (own_rows * row_scale * ffn_gain_ref[:, own_columns]).astype(
            narrow
        )
        flat[0:count, other_columns] = (
            other_half * row_scale * ffn_gain_ref[:, other_columns]
        ).astype(narrow)
        if chunk == 0:
            weights[0].wait()
            weights[1].wait()
        for start in range(0, hidden, tile):
            columns = slice(start, start + tile)

            def both(weight):
                return jnp.dot(
                    flat[0:count], weight[:, columns], preferred_element_type=jnp.float32
                )

            gated = jnp.minimum(both(gate_w), clamp_limit)
            raised = jnp.clip(both(up_w), -clamp_limit, clamp_limit) + 1.0
            activation[0:count, columns] = (
                raised * gated * (1.0 / (1.0 + jnp.exp(-swish_alpha * gated)))
            ).astype(jnp.bfloat16)
        if chunk == 0:
            weights[2].wait()
        part_send[chunk, 0:count] = jnp.dot(
            activation[0:count], down_w[:, other_columns], preferred_element_type=jnp.float32
        ).astype(jnp.bfloat16)
        to_pair(
            2,
            chunk,
            part_send.at[chunk, pl.ds(0, count)],
            part_recv.at[chunk, pl.ds(0, count)],
        )
        part_own[0:count] = jnp.dot(
            activation[0:count], down_w[:, own_columns], preferred_element_type=jnp.float32
        ).astype(jnp.bfloat16)
        pairs[2, chunk].wait_recv()
        back_send[first:last] = (
            (part_own[0:count].astype(jnp.float32) + part_recv[chunk, 0:count].astype(jnp.float32))
            .reshape(last - first, plane, capacity, half_width)
            .astype(jnp.bfloat16)
        )
        for step in range(last - 1, first - 1, -1):
            to_plane("back", step, back_send, back_recv)

    over_slots = (((0,), (0,)), ((), ()))

    def weigh(step):
        from_plane("back", step)
        returned = (
            back_recv[step].astype(jnp.float32).reshape(slots, half_width).astype(jnp.bfloat16)
        )
        high = combine_ref[step].astype(jnp.bfloat16)
        low = (combine_ref[step] - high.astype(jnp.float32)).astype(jnp.bfloat16)
        return lax.dot_general(
            high, returned, over_slots, preferred_element_type=jnp.float32
        ) + lax.dot_general(low, returned, over_slots, preferred_element_type=jnp.float32)

    def send_sum(step):
        sum_send[step] = weigh(step).astype(jnp.bfloat16)
        to_line("sum", sum_send.at[step], sum_recv.at[step], step)

    near = max(1, floors // 2)
    chunks = [(step, step + 1) for step in range(floors - 1, near - 1, -1)] + [(0, near)]
    for step in outer + [0]:
        share_mixed(step)
    for step in outer + [0]:
        project(step)
    for chunk, (first, last) in enumerate(chunks):
        apply_expert(chunk, first, last)
        if chunk:
            for step in range(chunks[chunk - 1][1] - 1, chunks[chunk - 1][0] - 1, -1):
                send_sum(step)
    for step in range(near - 1, 0, -1):
        send_sum(step)
    total = after_ref[...].astype(jnp.float32) + weigh(0)
    for step in range(1, floors):
        line_copies["sum", step].wait_recv()
        total = total + sum_recv[step].astype(jnp.float32)
    out_ref[...] = total.astype(jnp.bfloat16)
    for group in (line_copies, plane_copies, pairs):
        for copy in group.values():
            copy.wait_send()
    swap_rows.wait_send()
    swap_mixed.wait_send()


def layer_call(floors, group_channels, peers, capacity, residual, *operands):
    state, in_proj, push_map, read_map, out_proj, w_gate, w_up, w_down = operands[9:]
    row_count, half_width = residual.shape
    channels = in_proj.shape[1]
    plane = peers // floors
    slots = plane * capacity
    near = max(1, floors // 2)
    chunk_count = floors - near + 1
    rows = near * slots
    narrow = jnp.bfloat16
    wide_blocks = pltpu.VMEM((floors, plane, capacity, half_width), narrow)
    thin_blocks = pltpu.VMEM((floors, plane, capacity, channels), narrow)
    dma = pltpu.SemaphoreType.DMA
    vmem = pl.BlockSpec(memory_space=pltpu.VMEM)
    anywhere = pl.BlockSpec(memory_space=pl.ANY)
    return pl.pallas_call(
        functools.partial(layer_kernel, floors, peers, capacity, group_channels),
        out_shape=(
            pltpu.VMEM(residual.shape, narrow),
            pltpu.VMEM(state.shape, jnp.float32),
        ),
        in_specs=[vmem] * 10 + [anywhere] * 8,
        out_specs=(vmem, vmem),
        scratch_shapes=[
            pltpu.VMEM(in_proj.shape, narrow),
            pltpu.VMEM(push_map.shape, jnp.float32),
            pltpu.VMEM(read_map.shape, jnp.float32),
            pltpu.VMEM(out_proj.shape, narrow),
            pltpu.VMEM(residual.shape, narrow),
            pltpu.VMEM((row_count, channels), narrow),
            pltpu.VMEM(residual.shape, narrow),
            pltpu.VMEM((4, state.shape[2]), jnp.float32),
            pltpu.VMEM((floors, 2 * operands[0].shape[0], row_count), jnp.float32),
            pltpu.VMEM((floors, slots, row_count), narrow),
            pltpu.VMEM((floors, slots, row_count), jnp.float32),
            pltpu.VMEM((floors, row_count, half_width), narrow),
            pltpu.VMEM((floors, row_count, channels), narrow),
            wide_blocks,
            thin_blocks,
            wide_blocks,
            thin_blocks,
            thin_blocks,
            pltpu.VMEM((max(slots, row_count), 2 * channels), narrow),
            pltpu.VMEM((floors, slots, half_width), narrow),
            pltpu.VMEM((floors, slots, half_width), narrow),
            pltpu.VMEM(w_gate.shape, narrow),
            pltpu.VMEM(w_up.shape, narrow),
            pltpu.VMEM(w_down.shape, narrow),
            pltpu.VMEM((rows, 2 * half_width), narrow),
            pltpu.VMEM((rows, w_gate.shape[1]), narrow),
            pltpu.VMEM((chunk_count, rows, half_width), narrow),
            pltpu.VMEM((chunk_count, rows, half_width), narrow),
            pltpu.VMEM((rows, half_width), narrow),
            wide_blocks,
            wide_blocks,
            pltpu.VMEM((floors, row_count, half_width), narrow),
            pltpu.VMEM((floors, row_count, half_width), narrow),
            dma((3,)),
            dma((5,)),
            dma((2,)),
            dma((2,)),
            dma((4, floors)),
            dma((4, floors)),
            dma((3, floors)),
            dma((3, floors)),
            dma((3, floors, plane)),
            dma((3, floors, plane)),
        ],
        compiler_params=pltpu.CompilerParams(
            collective_id=0, has_side_effects=True, vmem_limit_bytes=56 * 1024 * 1024
        ),
    )(residual, *operands)


def local(
    floors,
    residual,
    route_ids,
    route_weights,
    carried_state,
    mix_gain,
    in_proj,
    decay_rate,
    frequency,
    step_size,
    input_map,
    output_matrix,
    passthrough_scale,
    out_gain,
    out_proj,
    ffn_gain,
    w_gate,
    w_up,
    w_down,
):
    row_count, half_width = residual.shape
    top_count = route_ids.shape[1]
    local_experts = w_gate.shape[0]
    peer_count = lax.axis_size("ep")
    expert_count = local_experts * peer_count
    capacity = max(2, 3 * row_count * top_count // (2 * expert_count))
    capacity = -(-capacity // 8) * 8
    push_map = jnp.swapaxes(input_map, 2, 3).reshape(2, -1, input_map.shape[2])
    read_map = output_matrix.reshape(2, -1, output_matrix.shape[3])
    updated, new_state = layer_call(
        floors,
        input_map.shape[3],
        peer_count,
        capacity,
        residual,
        route_ids.T,
        route_weights.T,
        mix_gain[None, :],
        decay_rate,
        frequency,
        step_size[None, :],
        passthrough_scale[None, :],
        out_gain[None, :],
        ffn_gain[None, :],
        carried_state,
        in_proj,
        push_map,
        read_map,
        out_proj,
        w_gate[0],
        w_up[0],
        w_down[0],
    )
    return (updated, new_state)


def floor_count(mesh):
    heights = {getattr(device, "coords", (0, 0, 0))[2] for device in mesh.devices.flat}
    return len(heights)


def solution(mesh):
    placed = (
        P("ep", "tp"),
        P("ep", None),
        P("ep", None),
        P(None, "ep", "tp"),
        P(),
        P(None, "tp"),
        P("tp", None),
        P("tp", None),
        P("tp"),
        P(None, "tp", None, None),
        P(None, "tp", None, None),
        P("tp"),
        P(),
        P(None, "tp"),
        P(),
        P("ep", None, "tp"),
        P("ep", None, "tp"),
        P("ep", "tp", None),
    )
    return jax.shard_map(
        functools.partial(local, floor_count(mesh)),
        mesh=mesh,
        in_specs=placed,
        out_specs=(P("ep", "tp"), P(None, "ep", "tp")),
        check_vma=False,
    )
```

time: 55.6 us -> 56.2 us (1.011)
  Pallas kernels: 53.2 us -> 53.8 us
    pallas_call x1, Pallas kernels: 53.2 us -> 53.8 us  [layer_call(): pl.pallas_call(functools.partial(layer_kernel, floors, peers, capacity, g...]
where the time goes in v2:
time: 56.2 us; the launch traced here: 56 us
  Pallas kernels  53.8 us (96%)
  local copies, waits for them, and re-layouts  1.63 us (3%)
  between operations  0.65 us (1%)
    pallas_call x1, Pallas kernels, layer_call(): pl.pallas_call(functools.partial(layer_kernel, floors, peers, capacity, g...  53.8 us
    unnamed x2, local copies, waits for them, and re-layouts  1.63 us

profile of v2, /device:TPU:0, one launch (start us, length us, event | category | flops | bytes accessed | tf_op | source)
XLA Modules:
  0.0 56.0 jit_solution(17863749411534546615)
XLA Ops:
  0.6 53.8 %shard_map.185 = (bf16[64,1024]{1,0:T(8,128)(2,1)S(1)}, f32[2,64,2048]{2,1,0:T(8,128)S(1)}) custom-call(bf16[64,1024]{1,0:T(8,128)(2,1)} %residual_ref.1, s32[4,64]{1,0:T(4,128)} %bitcast.22, f32[4,64]{1,0:T(4,128)} %bitcast.23, f32[1,2048]{1,0:T(1,128)} %bitcast.19, f32[32,64]{1,0:T(8,128)} %decay_ref.1, f32[32,64]{1,0:T(8,128)} %frequency_ref.1, ...), custom_call_target="tpu_custom_call" | custom-call | tf_op jit(solution)/shard_map/pallas_call | solution.py:541
  54.4 0.7 %copy.22 = bf16[64,1024]{1,0:T(8,128)(2,1)} copy(bf16[64,1024]{1,0:T(8,128)(2,1)S(1)} %get-tuple-element.2) | data formatting | bytes 262144
  55.1 1.0 %copy.23 = f32[2,64,2048]{2,1,0:T(8,128)} copy(f32[2,64,2048]{2,1,0:T(8,128)S(1)} %get-tuple-element.3) | data formatting | bytes 2097152

commit v3 on v1

--- a/solution.py
+++ b/solution.py
@@ -62,10 +62,10 @@
         )
 
 
-def fill_routes(capacity, ids_ref, route_weight_ref, taken_ref, combine_ref):
+def fill_routes(capacity, me, ids_ref, route_weight_ref, taken_ref, combine_ref):
     top_count, rows = ids_ref.shape
     experts = taken_ref.shape[0] // capacity
-    expert_iota = lax.broadcasted_iota(jnp.int32, (experts, rows), 0)
+    expert_iota = jnp.bitwise_xor(lax.broadcasted_iota(jnp.int32, (experts, rows), 0), me)
     chosen = jnp.zeros((experts, rows), jnp.float32)
     weight = jnp.zeros((experts, rows), jnp.float32)
     for choice in range(top_count):
@@ -94,6 +94,26 @@
     peers,
     capacity,
     group_channels,
+    residual_hbm,
+    ids_hbm,
+    route_weight_hbm,
+    mix_gain_hbm,
+    decay_hbm,
+    frequency_hbm,
+    step_hbm,
+    passthrough_hbm,
+    out_gain_hbm,
+    ffn_gain_hbm,
+    state_hbm,
+    in_hbm,
+    push_hbm,
+    read_hbm,
+    out_hbm,
+    gate_hbm,
+    up_hbm,
+    down_hbm,
+    out_ref,
+    state_v,
     residual_ref,
     ids_ref,
     route_weight_ref,
@@ -104,16 +124,6 @@
     passthrough_ref,
     out_gain_ref,
     ffn_gain_ref,
-    state_hbm,
-    in_hbm,
-    push_hbm,
-    read_hbm,
-    out_hbm,
-    gate_hbm,
-    up_hbm,
-    down_hbm,
-    out_ref,
-    state_v,
     in_v,
     push_v,
     read_v,
@@ -131,14 +141,14 @@
     down_w,
     rows_own,
     rows_other,
-    flat_own,
-    flat_other,
+    flat,
     activation,
     part_send,
     part_recv,
     part_own,
     back_send,
     back_recv,
+    small_sem,
     weight_sem,
     mixer_sem,
     swap_send_sem,
@@ -154,14 +164,35 @@
 ):
     me = lax.axis_index("ep")
     core = lax.axis_index("tp")
-    half_width = residual_ref.shape[1]
+    half_width = residual_hbm.shape[1]
     hidden = gate_w.shape[1]
-    tile = 256
+    tile = 1024
+    half_rows = residual_hbm.shape[1]
+    first_half = pl.ds(pl.multiple_of(core * half_rows, half_rows), half_rows)
+    second_half = pl.ds(pl.multiple_of((1 - core) * half_rows, half_rows), half_rows)
+    small_copies = [
+        pltpu.make_async_copy(source, target, small_sem.at[place])
+        for place, (source, target) in enumerate(
+            (
+                (residual_hbm, residual_ref),
+                (mix_gain_hbm, mix_gain_ref),
+                (ids_hbm, ids_ref),
+                (route_weight_hbm, route_weight_ref),
+                (decay_hbm, decay_ref),
+                (frequency_hbm, frequency_ref),
+                (step_hbm, step_ref),
+                (passthrough_hbm, passthrough_ref),
+                (out_gain_hbm, out_gain_ref),
+                (ffn_gain_hbm, ffn_gain_ref),
+            )
+        )
+    ]
     mixer_copies = [
         pltpu.make_async_copy(source, target, mixer_sem.at[place])
         for place, (source, target) in enumerate(
             (
-                (in_hbm, in_v),
+                (in_hbm.at[first_half], in_v.at[first_half]),
+                (in_hbm.at[second_half], in_v.at[second_half]),
                 (push_hbm, push_v),
                 (state_hbm, state_v),
                 (read_hbm, read_v),
@@ -174,7 +205,9 @@
         pltpu.make_async_copy(up_hbm, up_w, weight_sem.at[1]),
         pltpu.make_async_copy(down_hbm, down_w, weight_sem.at[2]),
     ]
-    for copy in mixer_copies:
+    for copy in small_copies:
+        copy.start()
+    for copy in mixer_copies[:6]:
         copy.start()
     barrier = pltpu.get_barrier_semaphore()
     for offset in range(1, peers):
@@ -187,8 +220,14 @@
     pl.semaphore_signal(
         barrier, inc=1, device_id=(me, 1 - core), device_id_type=pl.DeviceIdType.MESH
     )
+    for copy in small_copies[2:]:
+        copy.wait()
     fill_transition(decay_ref, frequency_ref, step_ref, transition_ref)
-    fill_routes(capacity, ids_ref, route_weight_ref, taken_ref, combine_ref)
+    fill_routes(capacity, me, ids_ref, route_weight_ref, taken_ref, combine_ref)
+    for copy in mixer_copies[6:]:
+        copy.start()
+    small_copies[0].wait()
+    small_copies[1].wait()
     pl.semaphore_wait(barrier, peers)
 
     def remote(source, target, send_sem, recv_sem, ep_index, tp_index):
@@ -215,6 +254,7 @@
     squares = row_squares(start_rows)
     mixer_copies[0].wait()
     channels_sum = jnp.dot(gained, in_v[own_columns, :], preferred_element_type=jnp.float32)
+    mixer_copies[1].wait()
     swap_rows.wait_recv()
     other_rows = residual_other[...].astype(jnp.float32)
     gained = (other_rows * mix_gain_ref[:, other_columns]).astype(narrow)
@@ -241,7 +281,7 @@
         values = source[part, start : start + wide, :]
         return jnp.where(inside, jnp.concatenate([values] * groups, axis=1), 0.0).astype(narrow)
 
-    for copy in mixer_copies[1:4]:
+    for copy in mixer_copies[2:5]:
         copy.wait()
     for place in range(mixer_width // wide):
         start = place * wide
@@ -289,7 +329,7 @@
     other_channels = pl.ds(pl.multiple_of((1 - core) * mixer_width, mixer_width), mixer_width)
     mine = mixer_own[...].astype(jnp.float32)
     squares = row_squares(mine)
-    mixer_copies[4].wait()
+    mixer_copies[5].wait()
     projected = jnp.dot(
         (mine * out_gain_ref[:, own_channels]).astype(narrow),
         out_v[own_channels, :],
@@ -307,31 +347,31 @@
         start_rows + projected * lax.rsqrt(squares / (2 * mixer_width) + epsilon)
     ).astype(narrow)
     after_ref[...] = after_rows
-    quarter = peers // 4
-    for place in range(4):
-        slots = slice(place * quarter * capacity, (place + 1) * quarter * capacity)
-        buffer_ref[place * quarter : (place + 1) * quarter] = (
+    half = peers // 2
+    middle = half + half // 2
+    chunks = ((half, middle), (middle, peers), (0, half))
+    pieces = ((half, middle), (middle, peers), (half // 2, half), (0, half // 2))
+    outward = {}
+    for first, last in pieces:
+        slots = slice(first * capacity, last * capacity)
+        buffer_ref[first:last] = (
             jnp.dot(taken_ref[slots, :], after_rows, preferred_element_type=jnp.float32)
-            .reshape(quarter, capacity, half_width)
+            .reshape(last - first, capacity, half_width)
             .astype(narrow)
         )
-
-    half = peers // 2
-    outward = {}
-    middle = half + half // 2
-    chunks = ((half, middle), (0, half), (middle, peers))
-    for offset in [one for span in chunks for one in range(*span) if one]:
-        peer = peer_of(me, offset)
-        outward[offset] = remote(
-            buffer_ref.at[peer],
-            rows_own.at[offset],
-            go_send_sem.at[offset],
-            go_recv_sem.at[offset],
-            peer,
-            core,
-        )
-        outward[offset].start()
-    rows_own[0] = buffer_ref[me]
+        for offset in range(first, last):
+            if not offset:
+                continue
+            outward[offset] = remote(
+                buffer_ref.at[offset],
+                rows_own.at[offset],
+                go_send_sem.at[offset],
+                go_recv_sem.at[offset],
+                peer_of(me, offset),
+                core,
+            )
+            outward[offset].start()
+    rows_own[0] = buffer_ref[0]
     back = {}
     parts = []
     pairs = {}
@@ -340,7 +380,7 @@
         for offset in range(first, last):
             if offset:
                 outward[offset].wait_recv()
-            source = rows_own.at[offset] if offset else buffer_ref.at[me]
+            source = rows_own.at[offset] if offset else buffer_ref.at[0]
             pairs[offset] = remote(
                 source,
                 rows_other.at[offset],
@@ -365,8 +405,8 @@
         row_scale = lax.rsqrt(
             (row_squares(own_rows) + row_squares(other_half)) / (2 * half_width) + epsilon
         )
-        flat_own[0:count] = (own_rows * row_scale * ffn_gain_ref[:, own_columns]).astype(narrow)
-        flat_other[0:count] = (other_half * row_scale * ffn_gain_ref[:, other_columns]).astype(narrow)
+        flat[0:count, own_columns] = (own_rows * row_scale * ffn_gain_ref[:, own_columns]).astype(narrow)
+        flat[0:count, other_columns] = (other_half * row_scale * ffn_gain_ref[:, other_columns]).astype(narrow)
         if chunk == 0:
             weights[0].wait()
             weights[1].wait()
@@ -376,13 +416,7 @@
 
             def both(weight):
                 return jnp.dot(
-                    flat_own[0:count],
-                    weight[pl.ds(own_start, half_width), columns],
-                    preferred_element_type=jnp.float32,
-                ) + jnp.dot(
-                    flat_other[0:count],
-                    weight[pl.ds(other_start, half_width), columns],
-                    preferred_element_type=jnp.float32,
+                    flat[0:count], weight[:, columns], preferred_element_type=jnp.float32
                 )
 
             gated = jnp.minimum(both(gate_w), clamp_limit)
@@ -428,33 +462,37 @@
         )
         for offset in range(first, last):
             if offset == 0:
-                back_recv[me] = back_send[0]
+                back_recv[0] = back_send[0]
                 continue
             peer = peer_of(me, offset)
             back[offset] = remote(
                 back_send.at[offset],
-                back_recv.at[me],
+                back_recv.at[offset],
                 back_send_sem.at[offset],
                 back_recv_sem.at[offset],
                 peer,
                 core,
             )
             back[offset].start()
-    for offset in range(1, peers):
-        back[offset].wait_recv()
-    returned = (
-        back_recv[...]
-        .astype(jnp.float32)
-        .reshape(peers * capacity, half_width)
-        .astype(jnp.bfloat16)
-    )
-    high = combine_ref[...].astype(jnp.bfloat16)
-    low = (combine_ref[...] - high.astype(jnp.float32)).astype(jnp.bfloat16)
     over_slots = (((0,), (0,)), ((), ()))
-    expert_sum = lax.dot_general(
-        high, returned, over_slots, preferred_element_type=jnp.float32
-    ) + lax.dot_general(low, returned, over_slots, preferred_element_type=jnp.float32)
-    out_ref[...] = (after_ref[...].astype(jnp.float32) + expert_sum).astype(jnp.bfloat16)
+    total = after_ref[...].astype(jnp.float32)
+    for first, last in chunks:
+        for offset in range(max(1, first), last):
+            back[offset].wait_recv()
+        returned = (
+            back_recv[first:last]
+            .astype(jnp.float32)
+            .reshape((last - first) * capacity, half_width)
+            .astype(jnp.bfloat16)
+        )
+        weight = combine_ref[first * capacity : last * capacity, :]
+        high = weight.astype(jnp.bfloat16)
+        low = (weight - high.astype(jnp.float32)).astype(jnp.bfloat16)
+        total = total + (
+            lax.dot_general(high, returned, over_slots, preferred_element_type=jnp.float32)
+            + lax.dot_general(low, returned, over_slots, preferred_element_type=jnp.float32)
+        )
+    out_ref[...] = total.astype(jnp.bfloat16)
     for offset in range(1, peers):
         outward[offset].wait_send()
         back[offset].wait_send()
@@ -483,9 +521,11 @@
             pltpu.VMEM(residual.shape, narrow),
             pltpu.VMEM(state.shape, jnp.float32),
         ),
-        in_specs=[vmem] * 10 + [anywhere] * 8,
+        in_specs=[anywhere] * 18,
         out_specs=(vmem, vmem),
         scratch_shapes=[
+            pltpu.VMEM(residual.shape, narrow),
+            *[pltpu.VMEM(one.shape, one.dtype) for one in operands[:9]],
             pltpu.VMEM(in_proj.shape, narrow),
             pltpu.VMEM(push_map.shape, jnp.float32),
             pltpu.VMEM(read_map.shape, jnp.float32),
@@ -503,16 +543,16 @@
             pltpu.VMEM(w_down.shape, narrow),
             blocks,
             blocks,
-            flat,
-            flat,
+            pltpu.VMEM((rows, 2 * half_width), narrow),
             pltpu.VMEM((rows, w_gate.shape[1]), narrow),
             pltpu.VMEM((3, rows, half_width), narrow),
             pltpu.VMEM((3, rows, half_width), narrow),
             flat,
             blocks,
             blocks,
+            dma((10,)),
             dma((3,)),
-            dma((5,)),
+            dma((6,)),
             dma((2,)),
             dma((2,)),
             dma((peers,)),

time: 55.6 us -> 51.7 us (0.930)
  Pallas kernels: 53.2 us -> 49.3 us
    pallas_call x1, Pallas kernels: 53.2 us -> 49.3 us  [layer_call(): pl.pallas_call(functools.partial(layer_kernel, peers, capacity, group_cha...]
where the time goes in v3:
time: 51.7 us; the launch traced here: 51.5 us
  Pallas kernels  49.3 us (95%)
  local copies, waits for them, and re-layouts  1.63 us (3%)
  between operations  0.65 us (1%)
    pallas_call x1, Pallas kernels, layer_call(): pl.pallas_call(functools.partial(layer_kernel, peers, capacity, group_cha...  49.3 us
    unnamed x2, local copies, waits for them, and re-layouts  1.63 us

profile of v3, /device:TPU:0, one launch (start us, length us, event | category | flops | bytes accessed | tf_op | source)
XLA Modules:
  0.0 51.5 jit_solution(8831544856086147619)
XLA Ops:
  0.6 49.3 %shard_map.185 = (bf16[64,1024]{1,0:T(8,128)(2,1)S(1)}, f32[2,64,2048]{2,1,0:T(8,128)S(1)}) custom-call(bf16[64,1024]{1,0:T(8,128)(2,1)} %residual_hbm.1, s32[4,64]{1,0:T(4,128)} %bitcast.22, f32[4,64]{1,0:T(4,128)} %bitcast.23, f32[1,2048]{1,0:T(1,128)} %bitcast.19, f32[32,64]{1,0:T(8,128)} %decay_hbm.1, f32[32,64]{1,0:T(8,128)} %frequency_hbm.1, ...), custom_call_target="tpu_custom_call" | custom-call | tf_op jit(solution)/shard_map/pallas_call | solution.py:518
  49.9 0.7 %copy.22 = bf16[64,1024]{1,0:T(8,128)(2,1)} copy(bf16[64,1024]{1,0:T(8,128)(2,1)S(1)} %get-tuple-element.2) | data formatting | bytes 262144
  50.6 1.0 %copy.23 = f32[2,64,2048]{2,1,0:T(8,128)} copy(f32[2,64,2048]{2,1,0:T(8,128)S(1)} %get-tuple-element.3) | data formatting | bytes 2097152

commit v4 on v3

--- a/solution.py
+++ b/solution.py
@@ -9,6 +9,9 @@
 epsilon = 1e-06
 clamp_limit = 7.0
 swish_alpha = 1.702
+
+
+line_order = (2, 3, 1, 0)
 
 
 def discretize(decay_rate, frequency, step_size):
@@ -65,7 +68,12 @@
 def fill_routes(capacity, me, ids_ref, route_weight_ref, taken_ref, combine_ref):
     top_count, rows = ids_ref.shape
     experts = taken_ref.shape[0] // capacity
-    expert_iota = jnp.bitwise_xor(lax.broadcasted_iota(jnp.int32, (experts, rows), 0), me)
+    place = lax.broadcasted_iota(jnp.int32, (experts, rows), 0)
+    quarter = experts // 4
+    block = jnp.zeros((experts, rows), jnp.int32)
+    for turn, line in enumerate(line_order):
+        block = jnp.where(place // quarter == turn, line, block)
+    expert_iota = jnp.bitwise_xor(block * quarter + place % quarter, me)
     chosen = jnp.zeros((experts, rows), jnp.float32)
     weight = jnp.zeros((experts, rows), jnp.float32)
     for choice in range(top_count):
@@ -347,49 +355,50 @@
         start_rows + projected * lax.rsqrt(squares / (2 * mixer_width) + epsilon)
     ).astype(narrow)
     after_ref[...] = after_rows
-    half = peers // 2
-    middle = half + half // 2
-    chunks = ((half, middle), (middle, peers), (0, half))
-    pieces = ((half, middle), (middle, peers), (half // 2, half), (0, half // 2))
+    quarter = peers // 4
+    offsets = [line * quarter + spot for line in line_order for spot in range(quarter)]
+    own_place = offsets.index(0)
+    chunks = tuple((first * quarter, last * quarter) for first, last in ((0, 1), (1, 3), (3, 4)))
     outward = {}
-    for first, last in pieces:
+    for block in (0, 1, 2, 3):
+        first, last = block * quarter, (block + 1) * quarter
         slots = slice(first * capacity, last * capacity)
         buffer_ref[first:last] = (
             jnp.dot(taken_ref[slots, :], after_rows, preferred_element_type=jnp.float32)
-            .reshape(last - first, capacity, half_width)
+            .reshape(quarter, capacity, half_width)
             .astype(narrow)
         )
-        for offset in range(first, last):
-            if not offset:
+        for place in range(first, last):
+            if place == own_place:
                 continue
-            outward[offset] = remote(
-                buffer_ref.at[offset],
-                rows_own.at[offset],
-                go_send_sem.at[offset],
-                go_recv_sem.at[offset],
-                peer_of(me, offset),
+            outward[place] = remote(
+                buffer_ref.at[place],
+                rows_own.at[place],
+                go_send_sem.at[place],
+                go_recv_sem.at[place],
+                peer_of(me, offsets[place]),
                 core,
             )
-            outward[offset].start()
-    rows_own[0] = buffer_ref[0]
+            outward[place].start()
+    rows_own[own_place] = buffer_ref[own_place]
     back = {}
     parts = []
     pairs = {}
     for chunk, (first, last) in enumerate(chunks):
         count = (last - first) * capacity
-        for offset in range(first, last):
-            if offset:
-                outward[offset].wait_recv()
-            source = rows_own.at[offset] if offset else buffer_ref.at[0]
-            pairs[offset] = remote(
+        for place in range(first, last):
+            if place != own_place:
+                outward[place].wait_recv()
+            source = rows_own.at[place] if place != own_place else buffer_ref.at[place]
+            pairs[place] = remote(
                 source,
-                rows_other.at[offset],
-                pair_send_sem.at[offset],
-                pair_recv_sem.at[offset],
+                rows_other.at[place],
+                pair_send_sem.at[place],
+                pair_recv_sem.at[place],
                 me,
                 1 - core,
             )
-            pairs[offset].start()
+            pairs[place].start()
         own_rows = (
             rows_own[first:last]
             .astype(jnp.float32)
@@ -460,25 +469,25 @@
             .reshape(last - first, capacity, half_width)
             .astype(jnp.bfloat16)
         )
-        for offset in range(first, last):
-            if offset == 0:
-                back_recv[0] = back_send[0]
+        for place in range(first, last):
+            if place == own_place:
+                back_recv[place] = back_send[place]
                 continue
-            peer = peer_of(me, offset)
-            back[offset] = remote(
-                back_send.at[offset],
-                back_recv.at[offset],
-                back_send_sem.at[offset],
-                back_recv_sem.at[offset],
-                peer,
+            back[place] = remote(
+                back_send.at[place],
+                back_recv.at[place],
+                back_send_sem.at[place],
+                back_recv_sem.at[place],
+                peer_of(me, offsets[place]),
                 core,
             )
-            back[offset].start()
+            back[place].start()
     over_slots = (((0,), (0,)), ((), ()))
     total = after_ref[...].astype(jnp.float32)
     for first, last in chunks:
-        for offset in range(max(1, first), last):
-            back[offset].wait_recv()
+        for place in range(first, last):
+            if place != own_place:
+                back[place].wait_recv()
         returned = (
             back_recv[first:last]
             .astype(jnp.float32)
@@ -493,9 +502,9 @@
             + lax.dot_general(low, returned, over_slots, preferred_element_type=jnp.float32)
         )
     out_ref[...] = total.astype(jnp.bfloat16)
-    for offset in range(1, peers):
-        outward[offset].wait_send()
-        back[offset].wait_send()
+    for place in outward:
+        outward[place].wait_send()
+        back[place].wait_send()
     for offset in range(peers):
         pairs[offset].wait_send()
     for copy in parts:

time: 51.7 us -> 51 us (0.986)
  Pallas kernels: 49.3 us -> 48.6 us
    pallas_call x1, Pallas kernels: 49.3 us -> 48.6 us  [layer_call(): pl.pallas_call(functools.partial(layer_kernel, peers, capacity, group_cha...]
where the time goes in v4:
time: 51 us; the launch traced here: 50.8 us
  Pallas kernels  48.6 us (95%)
  local copies, waits for them, and re-layouts  1.63 us (3%)
  between operations  0.65 us (1%)
    pallas_call x1, Pallas kernels, layer_call(): pl.pallas_call(functools.partial(layer_kernel, peers, capacity, group_cha...  48.6 us
    unnamed x2, local copies, waits for them, and re-layouts  1.63 us

profile of v4, /device:TPU:0, one launch (start us, length us, event | category | flops | bytes accessed | tf_op | source)
XLA Modules:
  0.0 50.8 jit_solution(12501999793177325335)
XLA Ops:
  0.6 48.6 %shard_map.185 = (bf16[64,1024]{1,0:T(8,128)(2,1)S(1)}, f32[2,64,2048]{2,1,0:T(8,128)S(1)}) custom-call(bf16[64,1024]{1,0:T(8,128)(2,1)} %residual_hbm.1, s32[4,64]{1,0:T(4,128)} %bitcast.22, f32[4,64]{1,0:T(4,128)} %bitcast.23, f32[1,2048]{1,0:T(1,128)} %bitcast.19, f32[32,64]{1,0:T(8,128)} %decay_hbm.1, f32[32,64]{1,0:T(8,128)} %frequency_hbm.1, ...), custom_call_target="tpu_custom_call" | custom-call | tf_op jit(solution)/shard_map/pallas_call | solution.py:527
  49.2 0.7 %copy.22 = bf16[64,1024]{1,0:T(8,128)(2,1)} copy(bf16[64,1024]{1,0:T(8,128)(2,1)S(1)} %get-tuple-element.2) | data formatting | bytes 262144
  49.9 1.0 %copy.23 = f32[2,64,2048]{2,1,0:T(8,128)} copy(f32[2,64,2048]{2,1,0:T(8,128)S(1)} %get-tuple-element.3) | data formatting | bytes 2097152
